TPU v7x, 32 devices: a whole 2x2x4 slice. The times are simulated.
32 devices in a mesh: sp: 8 (over z, x), tp: 4 (over y, core).
Axes of the slice: x: 2, y: 2, z: 4, core: 2. Of those that a mesh axis runs over, the one named last changes fastest.
Arguments:
- queries: bfloat16 [512, 16, 192], P('sp', 'tp'), may hold values from -400 to 400
- latents: bfloat16 [512, 512], P('sp'), may hold values from -6 to 6
- rope_keys: bfloat16 [512, 64], P('sp'), may hold values from -9 to 9
- latent_norm_scale: float32 [512], replicated, may hold values from 0.1 to 1.9
- key_value_weight: bfloat16 [512, 16, 256], P(None, 'tp'), may hold values from -0.25 to 0.25
- out_weight: bfloat16 [2048, 2048], P('tp'), may hold values from -1 to 1
- resid: bfloat16 [512, 2048], P('sp'), may hold values from -3 to 3
- ffn_gain: float32 [2048], replicated, may hold values from 0.1 to 1.9
- expert_ids: int32 [512, 2], P('sp'), may hold values from 0 to 7, all different within a row; in each aligned block of 64 rows (0 to 63, 64 to 127, ...) at most 24 rows name the same one
- route_weights: float32 [512, 2], P('sp'), may hold values from 0.1 to 1
- gate_weight: bfloat16 [8, 2048, 4096], P('sp', None, 'tp'), may hold values from -0.125 to 0.125
- up_weight: bfloat16 [8, 2048, 4096], P('sp', None, 'tp'), may hold values from -0.125 to 0.125
- down_weight: bfloat16 [8, 4096, 2048], P('sp', 'tp'), may hold values from -0.09375 to 0.09375
Outputs:
- updated: bfloat16 [512, 2048], P('sp', 'tp')
Inputs may be any that keep to these rules, and one draw needn't show every extreme that they name: `expert_ids`: among the rows of one device no expert is named more than 24 times, and in some devices some expert is named exactly 24 times.
All inputs are finite; a program needn't handle non-finite values.
Results may differ from a plain program's by a relative error of at most 0.025.
Values may be sent and summed in bfloat16 or wider, within the bound.
A program may use at most 64 MiB of HBM per device.

v0:
```python
import jax
import jax.numpy as jnp
from jax import lax
from jax.sharding import PartitionSpec as P

PLAIN_WIDTH = 128
VALUE_WIDTH = 128


rope_base = 10000.0
norm_eps = 1e-06


def rotary_table(positions, width):
    half_width = width // 2
    inverse = rope_base ** (-jnp.arange(half_width, dtype=jnp.float32) / half_width)
    turned = positions[:, None] * inverse[None, :]
    return (jnp.cos(turned), jnp.sin(turned))


def turn_pairs(vectors, cosines, sines):
    half_width = vectors.shape[-1] // 2
    front_half = vectors[..., :half_width]
    back_half = vectors[..., half_width:]
    return jnp.concatenate(
        [front_half * cosines - back_half * sines, back_half * cosines + front_half * sines],
        axis=-1,
    )


def rms_scaled(matrix, gain):
    floats = matrix.astype(jnp.float32)
    return floats * lax.rsqrt(jnp.mean(floats * floats, axis=-1, keepdims=True) + norm_eps) * gain


def attend(state_now, query_plain, query_turned, key_plain, key_turned, head_values):
    running, totals, accumulated = state_now
    score_scale = (query_plain.shape[-1] + query_turned.shape[-1]) ** (-0.5)
    scores = jnp.einsum("qhn,khn->hqk", query_plain, key_plain, preferred_element_type=jnp.float32)
    scores = (
        scores
        + jnp.einsum("qhr,kr->hqk", query_turned, key_turned, preferred_element_type=jnp.float32)
    ) * score_scale
    highest = jnp.max(scores, axis=-1)
    fade_by = jnp.exp(running - highest)
    exps = jnp.exp(scores - highest[..., None])
    totals = totals * fade_by + jnp.sum(exps, axis=-1)
    summed = jnp.einsum(
        "hqk,khv->qhv", exps.astype(jnp.bfloat16), head_values, preferred_element_type=jnp.float32
    )
    accumulated = accumulated * jnp.transpose(fade_by)[:, :, None] + summed
    return (highest, totals, accumulated)


def finish_expert(gate_act, up_act, down_matrix, senders, items):
    hidden = (jax.nn.silu(gate_act) * up_act).astype(jnp.bfloat16)
    partial_rows = jnp.dot(hidden, down_matrix, preferred_element_type=jnp.float32).reshape(
        senders, items, -1
    )
    col_share = lax.psum_scatter(
        partial_rows.astype(jnp.bfloat16), "tp", scatter_dimension=2, tiled=True
    )
    return lax.all_to_all(col_share, "sp", split_axis=0, concat_axis=0, tiled=True)


def shards(
    queries,
    latents,
    rope_keys,
    latent_norm_scale,
    key_value_weight,
    out_weight,
    resid,
    ffn_gain,
    expert_ids,
    route_weights,
    gate_weight,
    up_weight,
    down_weight,
):
    tok_rows, local_heads, _ = queries.shape
    offset = lax.axis_index("sp") * tok_rows
    positions = (offset + jnp.arange(tok_rows, dtype=jnp.int32)).astype(jnp.float32)
    cosines, sines = rotary_table(positions, rope_keys.shape[1])
    query_plain = queries[:, :, :PLAIN_WIDTH]
    query_turned = turn_pairs(
        queries[:, :, PLAIN_WIDTH:].astype(jnp.float32), cosines[:, None, :], sines[:, None, :]
    ).astype(jnp.bfloat16)
    key_turned = turn_pairs(rope_keys.astype(jnp.float32), cosines, sines).astype(jnp.bfloat16)
    normalized_latent = rms_scaled(latents, latent_norm_scale).astype(jnp.bfloat16)
    key_project = key_value_weight.reshape(key_value_weight.shape[0], -1)
    pair_rows = tok_rows // 2
    turned_pairs = key_turned.reshape(pair_rows, -1)
    start_state = (
        jnp.full((local_heads, tok_rows), -jnp.inf, jnp.float32),
        jnp.zeros((local_heads, tok_rows), jnp.float32),
        jnp.zeros((tok_rows, local_heads, VALUE_WIDTH), jnp.float32),
    )
    own_projected = jnp.dot(
        normalized_latent, key_project, preferred_element_type=jnp.float32
    ).astype(jnp.bfloat16)
    head_piece = lax.all_gather(own_projected.reshape(pair_rows, -1), "sp", axis=0, tiled=True)
    turned_piece = lax.all_gather(turned_pairs, "sp", axis=0, tiled=True)
    row_count = head_piece.shape[0] * 2
    projected_rows = head_piece.reshape(row_count, -1)
    per_head = projected_rows.reshape(row_count, local_heads, -1)
    key_plain = per_head[:, :, :PLAIN_WIDTH]
    head_values = per_head[:, :, PLAIN_WIDTH:]
    final_state = attend(
        start_state,
        query_plain,
        query_turned,
        key_plain,
        turned_piece.reshape(row_count, -1),
        head_values,
    )
    _, totals, accumulated = final_state
    attended = (accumulated / jnp.transpose(totals)[:, :, None]).astype(jnp.bfloat16)
    head_partial = jnp.dot(
        attended.reshape(tok_rows, -1), out_weight, preferred_element_type=jnp.float32
    )
    mixed = lax.psum(head_partial.astype(jnp.bfloat16), "tp").astype(jnp.float32)
    middle_float = (resid.astype(jnp.float32) + mixed).astype(jnp.bfloat16).astype(jnp.float32)
    normed = rms_scaled(middle_float, ffn_gain).astype(jnp.bfloat16)
    experts = lax.axis_size("sp")
    top_count = expert_ids.shape[1]
    capacity = (3 * tok_rows * top_count + 2 * experts - 1) // (2 * experts)
    flat_ids = expert_ids.reshape(-1)
    picked = (flat_ids[:, None] == jnp.arange(experts, dtype=jnp.int32)[None, :]).astype(jnp.int32)
    slot_rank = jnp.sum((jnp.cumsum(picked, axis=0) - picked) * picked, axis=1)
    slot_index = flat_ids * capacity + slot_rank
    sources = jnp.arange(flat_ids.shape[0], dtype=jnp.int32) // top_count
    owner_row = jnp.zeros((experts * capacity,), jnp.int32).at[slot_index].set(sources)
    filled = jnp.zeros((experts * capacity,), jnp.bool_).at[slot_index].set(True)
    outgoing = jnp.where(filled[:, None], normed[owner_row], jnp.zeros((), jnp.bfloat16)).reshape(
        experts, capacity, -1
    )
    arrived = lax.all_to_all(outgoing, "sp", split_axis=0, concat_axis=0, tiled=True)
    senders, items, width = arrived.shape
    rows_in = arrived.reshape(-1, width)
    gate_act = jnp.dot(rows_in, gate_weight[0], preferred_element_type=jnp.float32)
    up_act = jnp.dot(rows_in, up_weight[0], preferred_element_type=jnp.float32)
    returned = finish_expert(gate_act, up_act, down_weight[0], senders, items)
    columns = returned.shape[2]
    back_rows = returned.reshape(-1, columns)
    chosen_rows = back_rows[slot_index].astype(jnp.float32) * route_weights.reshape(-1)[:, None]
    routed = jnp.sum(chosen_rows.reshape(tok_rows, top_count, columns), axis=1)
    column_start = lax.axis_index("tp") * columns
    middle_cols = lax.dynamic_slice_in_dim(middle_float, column_start, columns, 1)
    return (middle_cols + routed).astype(jnp.bfloat16)


def solution(mesh):
    placed = (
        P("sp", "tp", None),
        P("sp", None),
        P("sp", None),
        P(),
        P(None, "tp", None),
        P("tp", None),
        P("sp", None),
        P(),
        P("sp", None),
        P("sp", None),
        P("sp", None, "tp"),
        P("sp", None, "tp"),
        P("sp", "tp", None),
    )
    return jax.shard_map(
        shards, mesh=mesh, in_specs=placed, out_specs=P("sp", "tp"), check_vma=False
    )
```

profile of v0, /device:TPU:0, one launch (start us, length us, event | category | flops | bytes accessed | tf_op | source)
XLA Modules:
  0.0 172.7 jit_solution(10261434299274544389)
XLA Ops:
  6.5 1.6 copy.35
  8.2 1.0 fusion.28
  9.1 1.2 convolution_convert_fusion.1
  10.3 0.7 reshape.151
  11.1 1.5 slice.25
  12.6 0.7 convert_element_type.75
  13.3 0.2 multiply_cosine_fusion
  13.5 0.1 pad_maximum_fusion
  13.6 0.1 convert_element_type.77
  13.7 32.5 %all_gather.7 = bf16[256,128]{1,0:T(8,128)(2,1)S(1)} all-gather(bf16[32,128]{1,0:T(8,128)(2,1)S(1)} %convert_element_type.77), channel_id=1, replica_groups=mesh['sp'=8,'tp'=4] {'sp'}, dimensions={0}, use_global_device_ids=true | all-gather | bytes 73728 | tf_op jit(solution)/shard_map/all_gather | solution.py:103
  46.2 0.1 reshape.152
  46.3 0.1 copy.26
  46.4 0.1 eq.15
  46.6 0.1 copy.25
  46.7 0.1 mul.175
  46.8 0.1 fusion.39
  46.9 0.2 reduce_window_sum.11
  47.1 0.2 select_reduce_fusion
  47.3 1.0 scatter_custom_fusion.1
  48.3 0.8 subtract_convert_fusion
  49.0 5.2 %all-gather.2.cloned.1.call-done = bf16[256,2048]{1,0:T(8,128)(2,1)} async-done(((bf16[32,2048]{1,0:T(8,128)(2,1)}), bf16[256,2048]{1,0:T(8,128)(2,1)}) %all-gather.2.cloned.1.call-update) | async-done | bytes 1048592 | tf_op jit(solution)/shard_map/all_gather | solution.py:102
  54.2 1.8 %reshape_reshape.3 = bf16[512,4,256]{2,1,0:T(4,128)(2,1)S(1)} reshape(bf16[256,2048]{1,0:T(8,128)(2,1)} %all-gather.2.cloned.1.call-done) | data formatting | bytes 2097152 | tf_op jit(solution)/shard_map/reshape;reshape | solution.py:106
  56.1 0.4 fusion.48
  56.5 1.1 convolution_bitcast_fusion.1
  57.6 1.2 fusion.49
  58.9 0.2 fusion.23
  59.1 0.3 fusion.20
  59.4 1.2 convolution_convert_fusion
  60.7 1.0 scatter_custom_fusion
  61.7 0.1 broadcast_in_dim.24
  61.8 29.9 %all-reduce.2.cloned.1.call-done = bf16[64,2048]{1,0:T(8,128)(2,1)} async-done(((bf16[64,2048]{1,0:T(8,128)(2,1)}), bf16[64,2048]{1,0:T(8,128)(2,1)}) %all-reduce.2.cloned.1.call-update) | async-done | bytes 262160 | tf_op jit(solution)/shard_map/psum | solution.py:122
  91.7 1.9 %fusion.26 = (f32[64,2048]{1,0:T(8,128)}, f32[64]{0:T(128)S(1)}) fusion(bf16[64,2048]{1,0:T(8,128)(2,1)} %all-reduce.2.cloned.1.call-done, bf16[64,2048]{1,0:T(8,128)(2,1)S(1)} %copy-done.1), kind=kLoop, calls=%fused_computation.33 | loop fusion | flops 917440 | bytes 1048832 | tf_op jit(solution)/shard_map/convert_element_type | solution.py:123
  93.7 1.1 multiply_convert_fusion
  94.8 1.1 gather_fusion
  95.9 0.1 broadcast_select_fusion
  96.1 24.6 %all_to_all.10 = bf16[8,24,2048]{2,1,0:T(8,128)(2,1)S(1)} all-to-all(bf16[8,24,2048]{2,1,0:T(8,128)(2,1)S(1)} %broadcast_select_fusion), channel_id=1, replica_groups=mesh['sp'=8,'tp'=4] {'sp'}, dimensions={0} | all-to-all | bytes 1572864 | tf_op jit(solution)/shard_map/all_to_all | solution.py:138
  120.6 3.2 %fusion.4 = f32[192,1024]{1,0:T(8,128)S(1)} fusion(bf16[192,2048]{1,0:T(8,128)(2,1)S(1)} %bitcast.69, bf16[1,2048,1024]{2,1,0:T(8,128)(2,1)} %param.23), kind=kOutput, calls=%fused_computation.8 | convolution fusion | flops 805306368 | bytes 5767168 | tf_op jit(solution)/shard_map/dot_general | solution.py:141
  123.9 1.1 fusion.12
  124.9 1.1 copy-done.6
  126.0 1.9 %fusion.6 = bf16[8,24,2048]{2,1,0:T(8,128)(2,1)} fusion(bf16[8,24,1024]{2,1,0:T(8,128)(2,1)S(1)} %bitcast.73, bf16[1,1024,2048]{2,1,0:T(8,128)(2,1)S(1)} %copy-done.6), kind=kOutput, calls=%fused_computation.10 | convolution fusion | flops 805699584 | bytes 5373952 | tf_op jit(solution)/shard_map/dot_general | solution.py:57
  128.0 22.0 %reduce-scatter.2.cloned.1.call-done = bf16[8,24,512]{2,1,0:T(8,128)(2,1)} async-done(((bf16[8,24,2048]{2,1,0:T(8,128)(2,1)}), bf16[8,24,512]{2,1,0:T(8,128)(2,1)}) %reduce-scatter.2.cloned.1.call-update) | async-done | bytes 196624 | tf_op jit(solution)/shard_map/reduce_scatter | solution.py:60
  149.9 5.5 %all-to-all-start.1 = ((bf16[8,24,512]{2,1,0:T(8,128)(2,1)}), bf16[8,24,512]{2,1,0:T(8,128)(2,1)S(1)}, u32[]{:S(2)}, u32[]{:S(2)}) async-start(bf16[8,24,512]{2,1,0:T(8,128)(2,1)} %reduce-scatter.2.cloned.1.call-done), calls=%async_computation.2 | async-start | bytes 393216 | tf_op jit(solution)/shard_map/all_to_all | solution.py:63
  155.4 0.1 copy.27
  155.5 7.7 %all-to-all-done.1 = bf16[8,24,512]{2,1,0:T(8,128)(2,1)S(1)} async-done(((bf16[8,24,512]{2,1,0:T(8,128)(2,1)}), bf16[8,24,512]{2,1,0:T(8,128)(2,1)S(1)}, u32[]{:S(2)}, u32[]{:S(2)}) %all-to-all-start.1) | async-done | bytes 196640 | tf_op jit(solution)/shard_map/all_to_all | solution.py:63
  163.2 0.8 gather_fusion.1
  164.1 0.2 reshape.156
  164.3 0.4 multiply_reduce_fusion.1
  164.6 1.6 add_convert_fusion.1
  (35 shorter events, 0.3 us)
Async XLA Ops:
  6.5 52.9 %copy-start = (bf16[512,2048]{1,0:T(8,128)(2,1)S(1)}, bf16[512,2048]{1,0:T(8,128)(2,1)}, u32[]{:S(2)}) copy-start(bf16[512,2048]{1,0:T(8,128)(2,1)} %param.18) | copy-start | bytes 6291460
  6.5 41.7 %slice-start = ((bf16[64,4,192]{2,1,0:T(4,128)(2,1)}), bf16[64,4,64]{2,1,0:T(4,128)(2,1)S(1)}, s32[]{:S(2)}) async-start(bf16[64,4,192]{2,1,0:T(4,128)(2,1)} %param.13), calls=%async_computation.6 | async-start | bytes 131072 | tf_op jit(solution)/shard_map/slice | solution.py:87
  6.5 39.8 %copy-start.3 = (s32[64,2]{0,1:T(2,128)S(1)}, s32[64,2]{0,1:T(2,128)}, u32[]{:S(2)}) copy-start(s32[64,2]{0,1:T(2,128)} %param.21) | copy-start | bytes 1540
  6.5 47.7 %all-gather.2.cloned.1.call-start = ((), (), s32[]{:S(2)}) async-start(), calls=%async_computation.3 | async-start | bytes 1179648 | tf_op jit(solution)/shard_map/all_gather | solution.py:102
  11.0 80.7 %all-reduce.2.cloned.1.call-start = ((), (), s32[]{:S(2)}) async-start(), calls=%async_computation.4 | async-start | bytes 524288 | tf_op jit(solution)/shard_map/psum | solution.py:122
  56.1 35.6 %copy-start.1 = (bf16[64,2048]{1,0:T(8,128)(2,1)S(1)}, bf16[64,2048]{1,0:T(8,128)(2,1)}, u32[]{:S(2)}) copy-start(bf16[64,2048]{1,0:T(8,128)(2,1)} %param.19) | copy-start | bytes 786436
  56.5 37.2 %copy-start.2 = (f32[2048]{0:T(1024)S(1)}, f32[2048]{0:T(1024)}, u32[]{:S(2)}) copy-start(f32[2048]{0:T(1024)} %param.20) | copy-start | bytes 24580
  60.6 89.3 %reduce-scatter.2.cloned.1.call-start = ((), (), s32[]{:S(2)}) async-start(), calls=%async_computation.5 | async-start | bytes 983040 | tf_op jit(solution)/shard_map/reduce_scatter | solution.py:60
  95.9 27.9 %copy-start.5 = (bf16[1,2048,1024]{2,1,0:T(8,128)(2,1)S(1)}, bf16[1,2048,1024]{2,1,0:T(8,128)(2,1)}, u32[]{:S(2)}) copy-start(bf16[1,2048,1024]{2,1,0:T(8,128)(2,1)} %param.24) | copy-start | bytes 12582916
  123.8 2.2 %copy-start.6 = (bf16[1,1024,2048]{2,1,0:T(8,128)(2,1)S(1)}, bf16[1,1024,2048]{2,1,0:T(8,128)(2,1)}, u32[]{:S(2)}) copy-start(bf16[1,1024,2048]{2,1,0:T(8,128)(2,1)} %param.25) | copy-start | bytes 12582916
  124.9 30.5 %copy-start.4 = (f32[64,2]{0,1:T(2,128)S(1)}, f32[64,2]{0,1:T(2,128)}, u32[]{:S(2)}) copy-start(f32[64,2]{0,1:T(2,128)} %param.22) | copy-start | bytes 1540
  149.9 13.3 %all-to-all-start.1 = ((bf16[8,24,512]{2,1,0:T(8,128)(2,1)}), bf16[8,24,512]{2,1,0:T(8,128)(2,1)S(1)}, u32[]{:S(2)}, u32[]{:S(2)}) async-start(bf16[8,24,512]{2,1,0:T(8,128)(2,1)} %reduce-scatter.2.cloned.1.call-done), calls=%async_computation.2 | async-start | bytes 393216 | tf_op jit(solution)/shard_map/all_to_all | solution.py:63
Sparse Core Ops, SparseCore 0:
  11.2 43.0 all-gather.1
  60.8 30.9 all-reduce.1
  128.1 21.7 reduce-scatter.1
where the time goes:
time: 173 us
  waiting for transfers between devices  64.8 us (37%)
  blocking collectives  57.1 us (33%)
  between operations  13.4 us (8%)
  local copies, waits for them, and re-layouts  12.1 us (7%)
  matrix products  11.2 us (6%)
  other arithmetic  8.52 us (5%)
  starting transfers between devices  5.6 us (3%)
    all_gather x1, blocking collectives, shards(): turned_piece = lax.all_gather(turned_pairs, 'sp', axis=0, tiled=True)  32.5 us
    psum x1, waiting for transfers between devices, shards(): lax.psum(head_partial.astype(jnp.bfloat16), 'tp').astype(jnp.float32)  29.9 us
    all_to_all x1, blocking collectives, shards(): lax.all_to_all(outgoing, 'sp', split_axis=0, concat_axis=0, tiled=True)  24.6 us
    reduce_scatter x1, waiting for transfers between devices, finish_expert(): lax.psum_scatter(partial_rows.astype(jnp.bfloat16), 'tp', scatter_dimensi...  22 us
    all_to_all x1, waiting for transfers between devices, finish_expert(): lax.all_to_all(col_share, 'sp', split_axis=0, concat_axis=0, tiled=True)  7.68 us
    all_to_all x1, starting transfers between devices, finish_expert(): lax.all_to_all(col_share, 'sp', split_axis=0, concat_axis=0, tiled=True)  5.52 us
    all_gather x1, waiting for transfers between devices, shards(): lax.all_gather(own_projected.reshape(pair_rows, -1), 'sp', axis=0, tiled=...  5.2 us
  transfers between devices with their start and end apart: 4, of which 4 were waited for; matrix products, arithmetic and copies ran while one was open for 4% of the time, Pallas kernels for 0%

commit v1 on v0

v1 whole, which is shorter than its diff:
```python
import functools

import jax
import jax.numpy as jnp
from jax import lax
from jax.experimental import pallas as pl
from jax.experimental.pallas import tpu as pltpu
from jax.sharding import PartitionSpec as P

PLAIN_WIDTH = 128
VALUE_WIDTH = 128
LANES = 128
MESH = pl.DeviceIdType.MESH

rope_base = 10000.0
norm_eps = 1e-06


def rotary_table(positions, width):
    half_width = width // 2
    inverse = rope_base ** (-jnp.arange(half_width, dtype=jnp.float32) / half_width)
    turned = positions[:, None] * inverse[None, :]
    return (jnp.cos(turned), jnp.sin(turned))


def turn_pairs(vectors, cosines, sines):
    half_width = vectors.shape[-1] // 2
    front_half = vectors[..., :half_width]
    back_half = vectors[..., half_width:]
    return jnp.concatenate(
        [front_half * cosines - back_half * sines, back_half * cosines + front_half * sines],
        axis=-1,
    )


def rms_scaled(matrix, gain):
    floats = matrix.astype(jnp.float32)
    return floats * lax.rsqrt(jnp.mean(floats * floats, axis=-1, keepdims=True) + norm_eps) * gain


def dot(a, b):
    return jnp.dot(a, b, preferred_element_type=jnp.float32)


def dot_nt(a, b):
    return lax.dot_general(a, b, (((1,), (1,)), ((), ())), preferred_element_type=jnp.float32)


def dot_tn(a, b):
    return lax.dot_general(a, b, (((0,), (0,)), ((), ())), preferred_element_type=jnp.float32)


def layer_kernel(
    cfg,
    query_ref,
    own_ref,
    resid_ref,
    gain_ref,
    ids_ref,
    route_ref,
    kv_hbm,
    ow_hbm,
    gate_hbm,
    up_hbm,
    down_hbm,
    out_ref,
    kv_w,
    ow_w,
    gate_w,
    up_w,
    down_w,
    lat_buf,
    att,
    mix_src,
    mix_buf,
    mid_src,
    mid_buf,
    rows_buf,
    hidden,
    pair_src,
    pair_buf,
    keep,
    sum_src,
    sum_buf,
    ret_src,
    ret_buf,
    load_sem,
    lat_sems,
    mid_sems,
    mix_sems,
    pair_sems,
    sum_sems,
    ret_sems,
):
    n_sp, n_tp, cap, tok, latent_width, rd, heads, top = cfg
    n_y = n_tp // 2
    cols = out_ref.shape[1]
    sp = lax.axis_index("sp")
    tp = lax.axis_index("tp")
    y = tp // 2
    core = lax.rem(tp, 2)
    partner = y * 2 + (1 - core)

    def sp_peer(d):
        return lax.rem(sp + d, n_sp)

    def tp_peer(d):
        return lax.rem(tp + d, n_tp)

    def y_peer(d):
        return lax.rem(y + d, n_y)

    def to(s, t):
        return {"sp": s, "tp": t}

    def loads():
        return [
            pltpu.make_async_copy(kv_hbm, kv_w, load_sem.at[0]),
            pltpu.make_async_copy(ow_hbm, ow_w, load_sem.at[1]),
            pltpu.make_async_copy(gate_hbm.at[0], gate_w, load_sem.at[2]),
            pltpu.make_async_copy(up_hbm.at[0], up_w, load_sem.at[3]),
            pltpu.make_async_copy(down_hbm.at[0], down_w, load_sem.at[4]),
        ]

    barrier = pltpu.get_barrier_semaphore()
    for d in range(1, n_sp):
        pl.semaphore_signal(barrier, inc=1, device_id=to(sp_peer(d), tp), device_id_type=MESH)
    for d in range(1, n_tp):
        pl.semaphore_signal(barrier, inc=1, device_id=to(sp, tp_peer(d)), device_id_type=MESH)
    weights = loads()
    for copy in weights:
        copy.start()
    pl.semaphore_wait(barrier, n_sp + n_tp - 2)

    def gather(source, buf, sems):
        a_send, a_recv, b_send, b_recv, c_send, c_recv = sems

        def a_copy(d, slot, s_to):
            return pltpu.make_async_remote_copy(
                src_ref=source(s_to),
                dst_ref=buf.at[slot, tp],
                send_sem=a_send.at[d],
                recv_sem=a_recv.at[slot],
                device_id=to(s_to, tp),
                device_id_type=MESH,
            )

        def b_copy(s, d):
            return pltpu.make_async_remote_copy(
                src_ref=buf.at[s, tp],
                dst_ref=buf.at[s, tp],
                send_sem=b_send.at[s, d],
                recv_sem=b_recv.at[s, y],
                device_id=to(sp, y_peer(d) * 2 + core),
                device_id_type=MESH,
            )

        def b_arrival(s, y_from):
            return pltpu.make_async_remote_copy(
                src_ref=buf.at[s, y_from * 2 + core],
                dst_ref=buf.at[s, y_from * 2 + core],
                send_sem=b_send.at[s, 0],
                recv_sem=b_recv.at[s, y_from],
                device_id=to(sp, partner),
                device_id_type=MESH,
            )

        def c_copy(s, y_of):
            return pltpu.make_async_remote_copy(
                src_ref=buf.at[s, y_of * 2 + core],
                dst_ref=buf.at[s, y_of * 2 + core],
                send_sem=c_send.at[s, y_of],
                recv_sem=c_recv.at[s, y_of],
                device_id=to(sp, partner),
                device_id_type=MESH,
            )

        def c_arrival(s, y_of):
            return pltpu.make_async_remote_copy(
                src_ref=buf.at[s, y_of * 2 + 1 - core],
                dst_ref=buf.at[s, y_of * 2 + 1 - core],
                send_sem=c_send.at[s, y_of],
                recv_sem=c_recv.at[s, y_of],
                device_id=to(sp, partner),
                device_id_type=MESH,
            )

        @pl.loop(1, n_sp)
        def _(d):
            a_copy(d, sp, sp_peer(d)).start()

        @pl.loop(0, n_sp)
        def _(d):
            s = lax.rem(sp + n_sp - d, n_sp)

            @pl.when(d > 0)
            def _():
                a_copy(d, s, sp_peer(d)).wait_recv()

            for step in range(1, n_y):
                b_copy(s, step).start()
            c_copy(s, y).start()

        @pl.loop(0, n_sp)
        def _(d):
            s = lax.rem(sp + n_sp - d, n_sp)
            for step in range(1, n_y):
                b_arrival(s, y_peer(step)).wait_recv()
                c_copy(s, y_peer(step)).start()

        @pl.loop(0, n_sp)
        def _(d):
            s = lax.rem(sp + n_sp - d, n_sp)
            for step in range(n_y):
                c_arrival(s, y_peer(step)).wait_recv()

        def drain():
            @pl.loop(0, n_sp)
            def _(d):
                @pl.when(d > 0)
                def _():
                    a_copy(d, sp, sp_peer(d)).wait_send()

                for step in range(1, n_y):
                    b_copy(d, step).wait_send()
                for step in range(n_y):
                    c_copy(d, y_peer(step)).wait_send()

        return drain

    own_copy = pltpu.make_async_copy(own_ref.at[tp], lat_buf.at[sp, tp], load_sem.at[5])
    own_copy.start()
    own_copy.wait()
    drain_lat = gather(lambda s_to: own_ref.at[tp], lat_buf, lat_sems)

    n_slots = n_sp * cap
    ids = ids_ref[...]
    expert_iota = lax.broadcasted_iota(jnp.int32, (tok, LANES), 1)
    picks = [(ids[:, k : k + 1] == expert_iota).astype(jnp.float32) for k in range(top)]
    picked = functools.reduce(lambda a, b: a + b, picks)
    earlier = (
        lax.broadcasted_iota(jnp.int32, (tok, tok), 0)
        > lax.broadcasted_iota(jnp.int32, (tok, tok), 1)
    ).astype(jnp.bfloat16)
    before = dot(earlier, picked.astype(jnp.bfloat16))
    slot_iota = lax.broadcasted_iota(jnp.int32, (tok, n_slots), 1)
    slots = []
    for k in range(top):
        rank = jnp.sum(before * picks[k], axis=1, keepdims=True).astype(jnp.int32)
        slots.append((slot_iota == ids[:, k : k + 1] * cap + rank).astype(jnp.float32))
    any_slot = functools.reduce(lambda a, b: a + b, slots)

    keys_all = n_sp * tok
    weights[0].wait()
    latents = lat_buf[:, :, :, :latent_width].reshape(keys_all, latent_width)
    turned = lat_buf[:, :, :, latent_width : latent_width + LANES].reshape(keys_all, LANES)
    scale = (PLAIN_WIDTH + rd) ** (-0.5)
    head_width = PLAIN_WIDTH + VALUE_WIDTH
    for h in range(heads):
        head_kv = dot(latents, kv_w[:, h * head_width : (h + 1) * head_width]).astype(jnp.bfloat16)
        query = query_ref[h]
        scores = dot_nt(query[:, :PLAIN_WIDTH], head_kv[:, :PLAIN_WIDTH])
        scores = (scores + dot_nt(query[:, PLAIN_WIDTH:], turned)) * scale
        exps = jnp.exp(scores - jnp.max(scores, axis=-1, keepdims=True))
        totals = jnp.sum(exps, axis=-1, keepdims=True)
        summed = dot(exps.astype(jnp.bfloat16), head_kv[:, PLAIN_WIDTH:])
        att[:, h * VALUE_WIDTH : (h + 1) * VALUE_WIDTH] = (summed / totals).astype(jnp.bfloat16)
    drain_lat()

    weights[1].wait()
    mix_send, mix_recv = mix_sems

    def out_part(t):
        return dot(att[...], ow_w[:, pl.ds(pl.multiple_of(t * cols, LANES), cols)])

    def mix_copy(d, t_from, t_to):
        return pltpu.make_async_remote_copy(
            src_ref=mix_src.at[d],
            dst_ref=mix_buf.at[t_from],
            send_sem=mix_send.at[d],
            recv_sem=mix_recv.at[t_from],
            device_id=to(sp, t_to),
            device_id_type=MESH,
        )

    @pl.loop(1, n_tp)
    def _(d):
        t_to = tp_peer(d)
        mix_src[d] = out_part(t_to).astype(jnp.bfloat16)
        mix_copy(d, tp, t_to).start()

    mixed = out_part(tp)
    for d in range(1, n_tp):
        t_from = tp_peer(d)
        mix_copy(d, t_from, t_from).wait_recv()
        mixed = mixed + mix_buf[t_from].astype(jnp.float32)
    own_cols = pl.ds(pl.multiple_of(tp * cols, LANES), cols)
    middle = (resid_ref[:, own_cols].astype(jnp.float32) + mixed).astype(jnp.bfloat16)

    outgoing = dot_tn(any_slot.astype(jnp.bfloat16), middle)
    for e in range(n_sp):
        mid_src[e] = outgoing[e * cap : (e + 1) * cap].astype(jnp.bfloat16)
    own_rows = pltpu.make_async_copy(mid_src.at[sp], mid_buf.at[sp, tp], load_sem.at[5])
    own_rows.start()
    own_rows.wait()
    drain_mid = gather(lambda s_to: mid_src.at[s_to], mid_buf, mid_sems)

    gain = gain_ref[...]
    normed = []
    for s in range(n_sp):
        whole = [mid_buf[s, t].astype(jnp.float32) for t in range(n_tp)]
        squares = functools.reduce(
            lambda a, b: a + b, [jnp.sum(w * w, axis=-1, keepdims=True) for w in whole]
        )
        inverse = lax.rsqrt(squares / (n_tp * cols) + norm_eps)
        normed.append(
            jnp.concatenate(
                [w * inverse * gain[:, t * cols : (t + 1) * cols] for t, w in enumerate(whole)],
                axis=1,
            )
        )
    rows_buf[...] = jnp.concatenate(normed, axis=0).astype(jnp.bfloat16)

    weights[2].wait()
    weights[3].wait()
    block = min(256, hidden.shape[1])

    @pl.loop(0, hidden.shape[1] // block)
    def _(j):
        here = pl.ds(pl.multiple_of(j * block, LANES), block)
        gate_act = dot(rows_buf[...], gate_w[:, here])
        up_act = dot(rows_buf[...], up_w[:, here])
        hidden[:, here] = (gate_act / (1.0 + jnp.exp(-gate_act)) * up_act).astype(jnp.bfloat16)

    drain_mid()
    for d in range(1, n_tp):
        mix_copy(d, tp, tp_peer(d)).wait_send()

    weights[4].wait()
    pair_send, pair_recv = pair_sems
    sum_send, sum_recv = sum_sems
    ret_send, ret_recv = ret_sems

    def down_part(t):
        return dot(hidden[...], down_w[:, pl.ds(pl.multiple_of(t * cols, LANES), cols)])

    def pair_copy(d):
        return pltpu.make_async_remote_copy(
            src_ref=pair_src.at[d],
            dst_ref=pair_buf.at[d],
            send_sem=pair_send.at[d],
            recv_sem=pair_recv.at[d],
            device_id=to(sp, partner),
            device_id_type=MESH,
        )

    def sum_copy(d, s, y_from, y_to):
        return pltpu.make_async_remote_copy(
            src_ref=sum_src.at[d, s],
            dst_ref=sum_buf.at[y_from, s],
            send_sem=sum_send.at[d, s],
            recv_sem=sum_recv.at[y_from, s],
            device_id=to(sp, y_to * 2 + core),
            device_id_type=MESH,
        )

    @pl.loop(0, n_y)
    def _(i):
        d = n_y - 1 - i
        part = down_part(y_peer(d) * 2 + 1 - core)
        for s in range(n_sp):
            pair_src[d, s] = part[s * cap : (s + 1) * cap].astype(jnp.bfloat16)
        pair_copy(d).start()
        keep[d] = down_part(y_peer(d) * 2 + core)

    @pl.loop(0, n_y - 1)
    def _(i):
        d = n_y - 1 - i
        pair_copy(d).wait_recv()
        for s in range(n_sp):
            sum_src[d, s] = (
                keep[d, s * cap : (s + 1) * cap] + pair_buf[d, s].astype(jnp.float32)
            ).astype(jnp.bfloat16)

        @pl.loop(0, n_sp)
        def _(k):
            sum_copy(d, sp_peer(k), y, y_peer(d)).start()

    pair_copy(0).wait_recv()

    def ret_copy(d, s_from, s_to):
        return pltpu.make_async_remote_copy(
            src_ref=ret_src.at[d],
            dst_ref=ret_buf.at[s_from],
            send_sem=ret_send.at[d],
            recv_sem=ret_recv.at[s_from],
            device_id=to(s_to, tp),
            device_id_type=MESH,
        )

    @pl.loop(0, n_sp)
    def _(i):
        d = lax.rem(i + 1, n_sp)
        s = sp_peer(d)
        total = keep[0, pl.ds(pl.multiple_of(s * cap, 8), cap)]
        total = total + pair_buf[0, s].astype(jnp.float32)
        for step in range(1, n_y):
            y_from = y_peer(step)
            sum_copy(step, s, y_from, y_from).wait_recv()
            total = total + sum_buf[y_from, s].astype(jnp.float32)
        ret_src[d] = total.astype(jnp.bfloat16)

        @pl.when(d > 0)
        def _():
            ret_copy(d, sp, s).start()

    own_back = pltpu.make_async_copy(ret_src.at[0], ret_buf.at[sp], load_sem.at[5])
    own_back.start()
    own_back.wait()

    @pl.loop(1, n_sp)
    def _(d):
        s_from = sp_peer(d)
        ret_copy(d, s_from, s_from).wait_recv()

    back = jnp.concatenate(
        [ret_buf[e].astype(jnp.float32) for e in range(n_sp)], axis=0
    ).astype(jnp.bfloat16)
    route = route_ref[...]
    routed = functools.reduce(
        lambda a, b: a + b,
        [dot(slots[k].astype(jnp.bfloat16), back) * route[:, k : k + 1] for k in range(top)],
    )
    out_ref[...] = (middle.astype(jnp.float32) + routed).astype(jnp.bfloat16)

    @pl.loop(0, n_y)
    def _(d):
        pair_copy(d).wait_send()

        @pl.when(d > 0)
        def _():
            @pl.loop(0, n_sp)
            def _(k):
                sum_copy(d, k, y, y_peer(d)).wait_send()

    @pl.loop(1, n_sp)
    def _(d):
        ret_copy(d, sp, sp_peer(d)).wait_send()


def shards(
    queries,
    latents,
    rope_keys,
    latent_norm_scale,
    key_value_weight,
    out_weight,
    resid,
    ffn_gain,
    expert_ids,
    route_weights,
    gate_weight,
    up_weight,
    down_weight,
):
    tok, heads, _ = queries.shape
    n_sp = lax.axis_size("sp")
    n_tp = lax.axis_size("tp")
    n_y = n_tp // 2
    width = resid.shape[1]
    latent_width = latents.shape[1]
    rd = rope_keys.shape[1]
    top = expert_ids.shape[1]
    cols = width // n_tp
    capacity = (3 * tok * top + 2 * n_sp - 1) // (2 * n_sp)
    cap = -(-capacity // 8) * 8
    ff = gate_weight.shape[2]

    positions = (lax.axis_index("sp") * tok + jnp.arange(tok, dtype=jnp.int32)).astype(jnp.float32)
    cosines, sines = rotary_table(positions, rd)
    lane_pad = LANES - rd
    query_turned = turn_pairs(
        queries[:, :, PLAIN_WIDTH:].astype(jnp.float32), cosines[:, None, :], sines[:, None, :]
    ).astype(jnp.bfloat16)
    query_all = jnp.concatenate(
        [
            queries[:, :, :PLAIN_WIDTH],
            query_turned,
            jnp.zeros((tok, heads, lane_pad), jnp.bfloat16),
        ],
        axis=2,
    ).transpose(1, 0, 2)
    key_turned = turn_pairs(rope_keys.astype(jnp.float32), cosines, sines).astype(jnp.bfloat16)
    own = jnp.concatenate(
        [
            rms_scaled(latents, latent_norm_scale).astype(jnp.bfloat16),
            key_turned,
            jnp.zeros((tok, lane_pad), jnp.bfloat16),
        ],
        axis=1,
    )
    own = own.reshape(n_tp, tok // n_tp, latent_width + LANES)

    vmem = pl.BlockSpec(memory_space=pltpu.VMEM)
    hbm = pl.BlockSpec(memory_space=pl.ANY)
    bf16, f32 = jnp.bfloat16, jnp.float32
    dma = pltpu.SemaphoreType.DMA

    def gather_sems():
        return (
            dma((n_sp,)),
            dma((n_sp,)),
            dma((n_sp, n_y)),
            dma((n_sp, n_y)),
            dma((n_sp, n_y)),
            dma((n_sp, n_y)),
        )

    scratch = [
        pltpu.VMEM((latent_width, heads * (PLAIN_WIDTH + VALUE_WIDTH)), bf16),
        pltpu.VMEM(out_weight.shape, bf16),
        pltpu.VMEM(gate_weight.shape[1:], bf16),
        pltpu.VMEM(up_weight.shape[1:], bf16),
        pltpu.VMEM(down_weight.shape[1:], bf16),
        pltpu.VMEM((n_sp,) + own.shape, bf16),
        pltpu.VMEM((tok, heads * VALUE_WIDTH), bf16),
        pltpu.VMEM((n_tp, tok, cols), bf16),
        pltpu.VMEM((n_tp, tok, cols), bf16),
        pltpu.VMEM((n_sp, cap, cols), bf16),
        pltpu.VMEM((n_sp, n_tp, cap, cols), bf16),
        pltpu.VMEM((n_sp * cap, width), bf16),
        pltpu.VMEM((n_sp * cap, ff), bf16),
        pltpu.VMEM((n_y, n_sp, cap, cols), bf16),
        pltpu.VMEM((n_y, n_sp, cap, cols), bf16),
        pltpu.VMEM((n_y, n_sp * cap, cols), f32),
        pltpu.VMEM((n_y, n_sp, cap, cols), bf16),
        pltpu.VMEM((n_y, n_sp, cap, cols), bf16),
        pltpu.VMEM((n_sp, cap, cols), bf16),
        pltpu.VMEM((n_sp, cap, cols), bf16),
        dma((6,)),
        gather_sems(),
        gather_sems(),
        (dma((n_tp,)), dma((n_tp,))),
        (dma((n_y,)), dma((n_y,))),
        (dma((n_y, n_sp)), dma((n_y, n_sp))),
        (dma((n_sp,)), dma((n_sp,))),
    ]
    cfg = (n_sp, n_tp, cap, tok, latent_width, rd, heads, top)
    return pl.pallas_call(
        functools.partial(layer_kernel, cfg),
        out_shape=jax.ShapeDtypeStruct((tok, cols), bf16),
        in_specs=[vmem] * 6 + [hbm] * 5,
        out_specs=vmem,
        scratch_shapes=scratch,
        compiler_params=pltpu.CompilerParams(
            collective_id=0, has_side_effects=True, vmem_limit_bytes=60 * 1024 * 1024
        ),
        name="layer",
    )(
        query_all,
        own,
        resid,
        ffn_gain.reshape(1, -1),
        expert_ids,
        route_weights,
        key_value_weight.reshape(latent_width, -1),
        out_weight,
        gate_weight,
        up_weight,
        down_weight,
    )


def solution(mesh):
    placed = (
        P("sp", "tp", None),
        P("sp", None),
        P("sp", None),
        P(),
        P(None, "tp", None),
        P("tp", None),
        P("sp", None),
        P(),
        P("sp", None),
        P("sp", None),
        P("sp", None, "tp"),
        P("sp", None, "tp"),
        P("sp", "tp", None),
    )
    return jax.shard_map(
        shards, mesh=mesh, in_specs=placed, out_specs=P("sp", "tp"), check_vma=False
    )
```

time: 173 us -> 64.9 us (0.38)
  waiting for transfers between devices: 64.8 us -> 0 us
  blocking collectives: 57.1 us -> 0 us
  Pallas kernels: 0 us -> 51.4 us
  between operations: 13.4 us -> 0.07 us
  matrix products: 11.2 us -> 0 us
  starting transfers between devices: 5.6 us -> 0 us
  other arithmetic: 8.52 us -> 4.39 us
  local copies, waits for them, and re-layouts: 12.1 us -> 8.57 us
    pallas_call x0 -> x1, Pallas kernels: none -> 51.4 us  [shards(): pl.pallas_call(functools.partial(layer_kernel, cfg), out_shape=jax.ShapeD...]
    all_gather x1 -> x0, blocking collectives: 32.5 us -> none  [shards(): turned_piece = lax.all_gather(turned_pairs, 'sp', axis=0, tiled=True)]
    psum x1 -> x0, waiting for transfers between devices: 29.9 us -> none  [shards(): lax.psum(head_partial.astype(jnp.bfloat16), 'tp').astype(jnp.float32)]
    all_to_all x1 -> x0, blocking collectives: 24.6 us -> none  [shards(): lax.all_to_all(outgoing, 'sp', split_axis=0, concat_axis=0, tiled=True)]
    reduce_scatter x1 -> x0, waiting for transfers between devices: 22 us -> none  [finish_expert(): lax.psum_scatter(partial_rows.astype(jnp.bfloat16), 'tp', scatter_dimensi...]
    dot_general x8 -> x0, matrix products: 11.2 us -> none  [the longest x1 3.2 us: shards(): jnp.dot(rows_in, gate_weight[0], preferred_element_type=jnp.float32)]
    all_to_all x1 -> x0, waiting for transfers between devices: 7.68 us -> none  [finish_expert(): lax.all_to_all(col_share, 'sp', split_axis=0, concat_axis=0, tiled=True)]
    all_to_all x1 -> x0, starting transfers between devices: 5.52 us -> none  [finish_expert(): lax.all_to_all(col_share, 'sp', split_axis=0, concat_axis=0, tiled=True)]
  transfers between devices with their start and end apart: 4 -> 0, of which waited for: 4 -> 0; matrix products, arithmetic and copies ran while one was open for 4% -> 0% of each run, Pallas kernels for 0% -> 0%
where the time goes in v1:
time: 64.9 us; the launch traced here: 64.4 us
  Pallas kernels  51.4 us (79%)
  local copies, waits for them, and re-layouts  8.57 us (13%)
  other arithmetic  4.39 us (7%)
    pallas_call x1, Pallas kernels, shards(): pl.pallas_call(functools.partial(layer_kernel, cfg), out_shape=jax.ShapeD...  51.4 us
    unnamed x5, local copies, waits for them, and re-layouts  6.68 us

profile of v1, /device:TPU:0, one launch (start us, length us, event | category | flops | bytes accessed | tf_op | source)
XLA Modules:
  0.0 64.4 jit_solution(2675470658010087376)
XLA Ops:
  0.0 0.1 pad.7.clone
  0.1 1.0 %fusion = f32[64]{0:T(128)S(1)} fusion(bf16[64,512]{1,0:T(8,128)(2,1)} %param.14), kind=kLoop, calls=%fused_computation.2 | loop fusion | flops 98240 | bytes 65792 | tf_op jit(solution)/shard_map/reduce_sum | solution.py:38
  1.1 0.1 pad.3.clone
  1.1 0.7 %convert_element_type.25 = f32[64,64]{1,0:T(8,128)S(1)} convert(bf16[64,64]{1,0:T(8,128)(2,1)} %param.15) | non-fusion elementwise | flops 4096 | bytes 24576 | tf_op jit(solution)/shard_map/convert_element_type | solution.py:493
  1.9 1.4 %copy.16.ids_ref = s32[64,2]{1,0:T(8,128)} copy(s32[64,2]{0,1:T(2,128)} %param.21) | data formatting | bytes 1024 | tf_op args[8]
  3.3 1.4 %copy.17.route_ref = f32[64,2]{1,0:T(8,128)} copy(f32[64,2]{0,1:T(2,128)} %param.22) | data formatting | bytes 1024 | tf_op args[9]
  4.6 0.2 subtract_convert_fusion.1
  4.8 0.9 %fusion.2 = bf16[64,512]{1,0:T(8,128)(2,1)S(1)} fusion(bf16[64,512]{1,0:T(8,128)(2,1)} %param.14, f32[512]{0:T(512)} %param.16, f32[64]{0:T(128)S(1)} %add_rsqrt_fusion), kind=kLoop, calls=%fused_computation.4 | loop fusion | flops 131072 | bytes 133376 | tf_op jit(solution)/shard_map/convert_element_type | solution.py:496
  5.8 0.7 %maximum_maximum_fusion = bf16[64,640]{1,0:T(8,128)(2,1)} fusion(bf16[64,32]{1,0:T(8,128)(2,1)S(1)} %get-tuple-element.8, bf16[64,32]{1,0:T(8,128)(2,1)S(1)} %get-tuple-element.7, bf16[64,512]{1,0:T(8,128)(2,1)S(1)} %fusion.2, bf16[640]{0:T(1024)(128)(2,1)S(1)} %pad.3.clone), kind=kLoop, calls=%fused_computation.8 | loop fusion | flops 327680 | bytes 156928 | tf_op jit(solution)/shard_map/concatenate | solution.py:494
  6.5 0.9 %slice.18 = bf16[64,4,128]{2,1,0:T(4,128)(2,1)S(1)} slice(bf16[64,4,192]{2,1,0:T(4,128)(2,1)} %param.13), slice={[0:64], [0:4], [0:128]} | slice | bytes 131072 | tf_op jit(solution)/shard_map/slice | solution.py:487
  7.4 0.9 %slice.19 = bf16[64,4,64]{2,1,0:T(4,128)(2,1)S(1)} slice(bf16[64,4,192]{2,1,0:T(4,128)(2,1)} %param.13), slice={[0:64], [0:4], [128:192]} | slice | bytes 65536 | tf_op jit(solution)/shard_map/slice | solution.py:483
  8.3 0.1 subtract_convert_fusion
  8.4 0.7 %maximum_bitcast_fusion.query_ref = bf16[4,64,256]{2,1,0:T(8,128)(2,1)} fusion(bf16[64,4,32]{2,0,1:T(8,128)(2,1)S(1)} %get-tuple-element.6, bf16[64,4,32]{2,0,1:T(8,128)(2,1)S(1)} %get-tuple-element.5, bf16[64,4,128]{2,0,1:T(8,128)(2,1)S(1)} %copy.18, bf16[256]{0:T(256)(128)(2,1)S(1)} %pad.7.clone), kind=kLoop, calls=%fused_computation.5 | loop fusion | flops 524288 | bytes 229888 | tf_op jit(solution)/shard_map/transpose | solution.py:492
  9.1 2.4 %copy.20 = bf16[64,8,4,256]{3,1,2,0:T(8,128)(2,1)} copy(bf16[64,8,4,256]{3,2,1,0:T(4,128)(2,1)} %bitcast.7) | data formatting | bytes 2097152
  11.6 51.4 %layer.1 = bf16[64,512]{1,0:T(8,128)(2,1)} custom-call(bf16[4,64,256]{2,1,0:T(8,128)(2,1)} %maximum_bitcast_fusion.query_ref, bf16[4,16,640]{2,1,0:T(8,128)(2,1)} %bitcast.8, bf16[64,2048]{1,0:T(8,128)(2,1)} %resid_ref.1, f32[1,2048]{1,0:T(1,128)} %bitcast.9, s32[64,2]{1,0:T(8,128)} %copy.16.ids_ref, f32[64,2]{1,0:T(8,128)} %copy.17.route_ref, ...), custom_call_target="tpu_custom_call" | custom-call | tf_op jit(solution)/shard_map/layer/pallas_call | solution.py:549
  63.0 1.5 %copy.23 = bf16[64,512]{1,0:T(8,128)(2,1)} copy(bf16[64,512]{1,0:T(8,128)(2,1)} %layer.1) | data formatting | bytes 131072
  (6 shorter events, 0.0 us)

commit v2 on v1

--- a/solution.py
+++ b/solution.py
@@ -18,24 +18,25 @@
 
 def rotary_table(positions, width):
     half_width = width // 2
-    inverse = rope_base ** (-jnp.arange(half_width, dtype=jnp.float32) / half_width)
-    turned = positions[:, None] * inverse[None, :]
-    return (jnp.cos(turned), jnp.sin(turned))
-
-
-def turn_pairs(vectors, cosines, sines):
+    lane = jnp.arange(width, dtype=jnp.int32)
+    power = (lane % half_width).astype(jnp.float32) / half_width
+    turned = positions[:, None] * (rope_base ** (-power))[None, :]
+    sign = jnp.where(lane < half_width, -1.0, 1.0).astype(jnp.float32)
+    return (jnp.cos(turned), jnp.sin(turned) * sign[None, :])
+
+
+def turn_pairs(vectors, cosines, signed_sines):
     half_width = vectors.shape[-1] // 2
-    front_half = vectors[..., :half_width]
-    back_half = vectors[..., half_width:]
-    return jnp.concatenate(
-        [front_half * cosines - back_half * sines, back_half * cosines + front_half * sines],
-        axis=-1,
+    swapped = jnp.concatenate([vectors[:, half_width:], vectors[:, :half_width]], axis=1)
+    return vectors * cosines + swapped * signed_sines
+
+
+def as_column(row):
+    size = row.shape[1]
+    same = lax.broadcasted_iota(jnp.int32, (size, size), 0) == lax.broadcasted_iota(
+        jnp.int32, (size, size), 1
     )
-
-
-def rms_scaled(matrix, gain):
-    floats = matrix.astype(jnp.float32)
-    return floats * lax.rsqrt(jnp.mean(floats * floats, axis=-1, keepdims=True) + norm_eps) * gain
+    return jnp.sum(jnp.where(same, jnp.broadcast_to(row, (size, size)), 0.0), axis=1, keepdims=True)
 
 
 def dot(a, b):
@@ -53,7 +54,11 @@
 def layer_kernel(
     cfg,
     query_ref,
-    own_ref,
+    latent_ref,
+    rope_ref,
+    scale_ref,
+    cos_ref,
+    sin_ref,
     resid_ref,
     gain_ref,
     ids_ref,
@@ -64,6 +69,9 @@
     up_hbm,
     down_hbm,
     out_ref,
+    own_ref,
+    query_w,
+    kv_raw,
     kv_w,
     ow_w,
     gate_w,
@@ -115,7 +123,7 @@
 
     def loads():
         return [
-            pltpu.make_async_copy(kv_hbm, kv_w, load_sem.at[0]),
+            pltpu.make_async_copy(kv_hbm, kv_raw, load_sem.at[0]),
             pltpu.make_async_copy(ow_hbm, ow_w, load_sem.at[1]),
             pltpu.make_async_copy(gate_hbm.at[0], gate_w, load_sem.at[2]),
             pltpu.make_async_copy(up_hbm.at[0], up_w, load_sem.at[3]),
@@ -130,9 +138,21 @@
     weights = loads()
     for copy in weights:
         copy.start()
+
+    latent_rows = latent_ref[...].astype(jnp.float32)
+    mean_square = jnp.mean(latent_rows * latent_rows, axis=-1, keepdims=True)
+    latent_rows = latent_rows * lax.rsqrt(mean_square + norm_eps) * scale_ref[...]
+    cosines, signed_sines = cos_ref[...], sin_ref[...]
+    key_rows = turn_pairs(rope_ref[...].astype(jnp.float32), cosines, signed_sines)
+    piece = tok // n_tp
+    for t in range(n_tp):
+        here = slice(t * piece, (t + 1) * piece)
+        own_ref[t, :, :latent_width] = latent_rows[here].astype(jnp.bfloat16)
+        own_ref[t, :, latent_width : latent_width + rd] = key_rows[here].astype(jnp.bfloat16)
+        own_ref[t, :, latent_width + rd :] = jnp.zeros((piece, LANES - rd), jnp.bfloat16)
     pl.semaphore_wait(barrier, n_sp + n_tp - 2)
 
-    def gather(source, buf, sems):
+    def gather(source, buf, sems, meanwhile=None):
         a_send, a_recv, b_send, b_recv, c_send, c_recv = sems
 
         def a_copy(d, slot, s_to):
@@ -189,6 +209,9 @@
         def _(d):
             a_copy(d, sp, sp_peer(d)).start()
 
+        if meanwhile is not None:
+            meanwhile()
+
         @pl.loop(0, n_sp)
         def _(d):
             s = lax.rem(sp + n_sp - d, n_sp)
@@ -228,37 +251,54 @@
 
         return drain
 
-    own_copy = pltpu.make_async_copy(own_ref.at[tp], lat_buf.at[sp, tp], load_sem.at[5])
-    own_copy.start()
-    own_copy.wait()
-    drain_lat = gather(lambda s_to: own_ref.at[tp], lat_buf, lat_sems)
-
-    n_slots = n_sp * cap
-    ids = ids_ref[...]
-    expert_iota = lax.broadcasted_iota(jnp.int32, (tok, LANES), 1)
-    picks = [(ids[:, k : k + 1] == expert_iota).astype(jnp.float32) for k in range(top)]
-    picked = functools.reduce(lambda a, b: a + b, picks)
-    earlier = (
-        lax.broadcasted_iota(jnp.int32, (tok, tok), 0)
-        > lax.broadcasted_iota(jnp.int32, (tok, tok), 1)
-    ).astype(jnp.bfloat16)
-    before = dot(earlier, picked.astype(jnp.bfloat16))
-    slot_iota = lax.broadcasted_iota(jnp.int32, (tok, n_slots), 1)
-    slots = []
-    for k in range(top):
-        rank = jnp.sum(before * picks[k], axis=1, keepdims=True).astype(jnp.int32)
-        slots.append((slot_iota == ids[:, k : k + 1] * cap + rank).astype(jnp.float32))
-    any_slot = functools.reduce(lambda a, b: a + b, slots)
+    lat_buf[sp, tp] = own_ref[tp]
+
+    head_width = PLAIN_WIDTH + VALUE_WIDTH
+
+    routing = []
+
+    def turn_queries():
+        for h in range(heads):
+            plain = query_ref[:, h, :PLAIN_WIDTH]
+            rotated = query_ref[:, h, PLAIN_WIDTH:].astype(jnp.float32)
+            query_w[h, :, :PLAIN_WIDTH] = plain
+            query_w[h, :, PLAIN_WIDTH : PLAIN_WIDTH + rd] = turn_pairs(
+                rotated, cosines, signed_sines
+            ).astype(jnp.bfloat16)
+            query_w[h, :, PLAIN_WIDTH + rd :] = jnp.zeros((tok, LANES - rd), jnp.bfloat16)
+
+        weights[0].wait()
+        for h in range(heads):
+            kv_w[:, h * head_width : (h + 1) * head_width] = kv_raw[:, h, :]
+        n_slots = n_sp * cap
+        ids = [as_column(ids_ref[k : k + 1, :].astype(jnp.float32)).astype(jnp.int32) for k in range(top)]
+        expert_iota = lax.broadcasted_iota(jnp.int32, (tok, LANES), 1)
+        picks = [(ids[k] == expert_iota).astype(jnp.float32) for k in range(top)]
+        picked = functools.reduce(lambda a, b: a + b, picks)
+        earlier = (
+            lax.broadcasted_iota(jnp.int32, (tok, tok), 0)
+            > lax.broadcasted_iota(jnp.int32, (tok, tok), 1)
+        ).astype(jnp.bfloat16)
+        before = dot(earlier, picked.astype(jnp.bfloat16))
+        slot_iota = lax.broadcasted_iota(jnp.int32, (tok, n_slots), 1)
+        slots = []
+        for k in range(top):
+            rank = jnp.sum(before * picks[k], axis=1, keepdims=True).astype(jnp.int32)
+            slots.append((slot_iota == ids[k] * cap + rank).astype(jnp.float32))
+        any_slot = functools.reduce(lambda a, b: a + b, slots)
+        routing.extend(slots + [any_slot])
+
+    drain_lat = gather(lambda s_to: own_ref.at[tp], lat_buf, lat_sems, turn_queries)
+
+    *slots, any_slot = routing
 
     keys_all = n_sp * tok
-    weights[0].wait()
     latents = lat_buf[:, :, :, :latent_width].reshape(keys_all, latent_width)
     turned = lat_buf[:, :, :, latent_width : latent_width + LANES].reshape(keys_all, LANES)
     scale = (PLAIN_WIDTH + rd) ** (-0.5)
-    head_width = PLAIN_WIDTH + VALUE_WIDTH
     for h in range(heads):
         head_kv = dot(latents, kv_w[:, h * head_width : (h + 1) * head_width]).astype(jnp.bfloat16)
-        query = query_ref[h]
+        query = query_w[h]
         scores = dot_nt(query[:, :PLAIN_WIDTH], head_kv[:, :PLAIN_WIDTH])
         scores = (scores + dot_nt(query[:, PLAIN_WIDTH:], turned)) * scale
         exps = jnp.exp(scores - jnp.max(scores, axis=-1, keepdims=True))
@@ -300,9 +340,7 @@
     outgoing = dot_tn(any_slot.astype(jnp.bfloat16), middle)
     for e in range(n_sp):
         mid_src[e] = outgoing[e * cap : (e + 1) * cap].astype(jnp.bfloat16)
-    own_rows = pltpu.make_async_copy(mid_src.at[sp], mid_buf.at[sp, tp], load_sem.at[5])
-    own_rows.start()
-    own_rows.wait()
+    mid_buf[sp, tp] = mid_src[sp]
     drain_mid = gather(lambda s_to: mid_src.at[s_to], mid_buf, mid_sems)
 
     gain = gain_ref[...]
@@ -384,7 +422,7 @@
 
         @pl.loop(0, n_sp)
         def _(k):
-            sum_copy(d, sp_peer(k), y, y_peer(d)).start()
+            sum_copy(d, sp_peer(lax.rem(k + 1, n_sp)), y, y_peer(d)).start()
 
     pair_copy(0).wait_recv()
 
@@ -414,9 +452,7 @@
         def _():
             ret_copy(d, sp, s).start()
 
-    own_back = pltpu.make_async_copy(ret_src.at[0], ret_buf.at[sp], load_sem.at[5])
-    own_back.start()
-    own_back.wait()
+    ret_buf[sp] = ret_src[0]
 
     @pl.loop(1, n_sp)
     def _(d):
@@ -426,10 +462,9 @@
     back = jnp.concatenate(
         [ret_buf[e].astype(jnp.float32) for e in range(n_sp)], axis=0
     ).astype(jnp.bfloat16)
-    route = route_ref[...]
     routed = functools.reduce(
         lambda a, b: a + b,
-        [dot(slots[k].astype(jnp.bfloat16), back) * route[:, k : k + 1] for k in range(top)],
+        [dot(slots[k].astype(jnp.bfloat16), back) * as_column(route_ref[k : k + 1, :]) for k in range(top)],
     )
     out_ref[...] = (middle.astype(jnp.float32) + routed).astype(jnp.bfloat16)
 
@@ -477,29 +512,7 @@
     ff = gate_weight.shape[2]
 
     positions = (lax.axis_index("sp") * tok + jnp.arange(tok, dtype=jnp.int32)).astype(jnp.float32)
-    cosines, sines = rotary_table(positions, rd)
-    lane_pad = LANES - rd
-    query_turned = turn_pairs(
-        queries[:, :, PLAIN_WIDTH:].astype(jnp.float32), cosines[:, None, :], sines[:, None, :]
-    ).astype(jnp.bfloat16)
-    query_all = jnp.concatenate(
-        [
-            queries[:, :, :PLAIN_WIDTH],
-            query_turned,
-            jnp.zeros((tok, heads, lane_pad), jnp.bfloat16),
-        ],
-        axis=2,
-    ).transpose(1, 0, 2)
-    key_turned = turn_pairs(rope_keys.astype(jnp.float32), cosines, sines).astype(jnp.bfloat16)
-    own = jnp.concatenate(
-        [
-            rms_scaled(latents, latent_norm_scale).astype(jnp.bfloat16),
-            key_turned,
-            jnp.zeros((tok, lane_pad), jnp.bfloat16),
-        ],
-        axis=1,
-    )
-    own = own.reshape(n_tp, tok // n_tp, latent_width + LANES)
+    cosines, signed_sines = rotary_table(positions, rd)
 
     vmem = pl.BlockSpec(memory_space=pltpu.VMEM)
     hbm = pl.BlockSpec(memory_space=pl.ANY)
@@ -516,13 +529,17 @@
             dma((n_sp, n_y)),
         )
 
+    own_shape = (n_tp, tok // n_tp, latent_width + LANES)
     scratch = [
+        pltpu.VMEM(own_shape, bf16),
+        pltpu.VMEM((heads, tok, PLAIN_WIDTH + LANES), bf16),
+        pltpu.VMEM((latent_width, heads, PLAIN_WIDTH + VALUE_WIDTH), bf16),
         pltpu.VMEM((latent_width, heads * (PLAIN_WIDTH + VALUE_WIDTH)), bf16),
         pltpu.VMEM(out_weight.shape, bf16),
         pltpu.VMEM(gate_weight.shape[1:], bf16),
         pltpu.VMEM(up_weight.shape[1:], bf16),
         pltpu.VMEM(down_weight.shape[1:], bf16),
-        pltpu.VMEM((n_sp,) + own.shape, bf16),
+        pltpu.VMEM((n_sp,) + own_shape, bf16),
         pltpu.VMEM((tok, heads * VALUE_WIDTH), bf16),
         pltpu.VMEM((n_tp, tok, cols), bf16),
         pltpu.VMEM((n_tp, tok, cols), bf16),
@@ -537,7 +554,7 @@
         pltpu.VMEM((n_y, n_sp, cap, cols), bf16),
         pltpu.VMEM((n_sp, cap, cols), bf16),
         pltpu.VMEM((n_sp, cap, cols), bf16),
-        dma((6,)),
+        dma((5,)),
         gather_sems(),
         gather_sems(),
         (dma((n_tp,)), dma((n_tp,))),
@@ -549,7 +566,7 @@
     return pl.pallas_call(
         functools.partial(layer_kernel, cfg),
         out_shape=jax.ShapeDtypeStruct((tok, cols), bf16),
-        in_specs=[vmem] * 6 + [hbm] * 5,
+        in_specs=[vmem] * 10 + [hbm] * 5,
         out_specs=vmem,
         scratch_shapes=scratch,
         compiler_params=pltpu.CompilerParams(
@@ -557,13 +574,17 @@
         ),
         name="layer",
     )(
-        query_all,
-        own,
+        queries,
+        latents,
+        rope_keys,
+        latent_norm_scale.reshape(1, -1),
+        cosines,
+        signed_sines,
         resid,
         ffn_gain.reshape(1, -1),
-        expert_ids,
-        route_weights,
-        key_value_weight.reshape(latent_width, -1),
+        expert_ids.T,
+        route_weights.T,
+        key_value_weight,
         out_weight,
         gate_weight,
         up_weight,

time: 64.9 us -> 53.3 us (0.82)
  local copies, waits for them, and re-layouts: 8.57 us -> 1.47 us
  other arithmetic: 4.39 us -> 0.84 us
    unnamed x5 -> x1, local copies, waits for them, and re-layouts: 6.68 us -> 1.47 us
    slice x2 -> x0, local copies, waits for them, and re-layouts: 1.73 us -> none  [the longest x1 0.87 us: shards(): queries[:, :, PLAIN_WIDTH:].astype(jnp.float32)]
    convert_element_type x3 -> x0, other arithmetic: 1.67 us -> none  [the longest x1 0.92 us: shards(): rms_scaled(latents, latent_norm_scale).astype(jnp.bfloat16)]
    reduce_sum x1 -> x0, other arithmetic: 0.95 us -> none  [rms_scaled(): jnp.mean(floats * floats, axis=-1, keepdims=True) + norm_eps]
    mul x0 -> x1, other arithmetic: none -> 0.83 us  [rotary_table(): return (jnp.cos(turned), jnp.sin(turned) * sign[None, :])]
    transpose x1 -> x0, other arithmetic: 0.74 us -> none  [shards(): query_all = jnp.concatenate([queries[:, :, :PLAIN_WIDTH], query_turned, j...]
    concatenate x1 -> x0, other arithmetic: 0.72 us -> none  [shards(): jnp.concatenate([rms_scaled(latents, latent_norm_scale).astype(jnp.bfloat...]
where the time goes in v2:
time: 53.3 us; the launch traced here: 53.1 us
  Pallas kernels  50.8 us (95%)
  local copies, waits for them, and re-layouts  1.47 us (3%)
  other arithmetic  0.84 us (2%)
    pallas_call x1, Pallas kernels, shards(): pl.pallas_call(functools.partial(layer_kernel, cfg), out_shape=jax.ShapeD...  50.8 us
    unnamed x1, local copies, waits for them, and re-layouts  1.47 us

profile of v2, /device:TPU:0, one launch (start us, length us, event | category | flops | bytes accessed | tf_op | source)
XLA Modules:
  0.0 53.1 jit_solution(1521539602289421477)
XLA Ops:
  0.0 0.8 %fusion = (f32[64,64]{1,0:T(8,128)}, f32[64,64]{1,0:T(8,128)}) fusion(f32[64]{0:T(128)S(1)} %get-tuple-element.7, f32[64]{0:T(128)S(1)} %get-tuple-element.8, f32[64]{0:T(128)S(1)} %add_convert_fusion), kind=kLoop, calls=%fused_computation.2 | loop fusion | flops 8192 | bytes 33536 | tf_op jit(solution)/shard_map/mul | solution.py:25
  0.8 50.8 %layer.1 = bf16[64,512]{1,0:T(8,128)(2,1)} custom-call(bf16[64,4,192]{2,1,0:T(4,128)(2,1)} %query_ref.1, bf16[64,512]{1,0:T(8,128)(2,1)} %latent_ref.1, bf16[64,64]{1,0:T(8,128)(2,1)} %rope_ref.1, f32[1,512]{1,0:T(1,128)} %bitcast.5, f32[64,64]{1,0:T(8,128)} %get-tuple-element.6.cos_ref, f32[64,64]{1,0:T(8,128)} %get-tuple-element.5.sin_ref, ...), custom_call_target="tpu_custom_call" | custom-call | tf_op jit(solution)/shard_map/layer/pallas_call | solution.py:566
  51.6 1.5 %copy.15 = bf16[64,512]{1,0:T(8,128)(2,1)} copy(bf16[64,512]{1,0:T(8,128)(2,1)} %layer.1) | data formatting | bytes 131072
  (2 shorter events, 0.0 us)
